TPU v7x, 32 devices: a whole 2x2x4 slice. The times are simulated.
32 devices in a mesh: ep: 8 (over z, x), tp: 4 (over y, core).
Axes of the slice: x: 2, y: 2, z: 4, core: 2. Of those that a mesh axis runs over, the one named last changes fastest.
Arguments:
- q_in: bfloat16 [4096, 1024], P('ep', 'tp'), may hold values from -6 to 6
- k_in: bfloat16 [4096, 256], P('ep'), may hold values from -6 to 6
- v_in: bfloat16 [4096, 256], P('ep'), may hold values from -6 to 6
- q_gain: float32 [64], replicated, may hold values from 0.1 to 1.9
- k_gain: float32 [64], replicated, may hold values from 0.1 to 1.9
- w_out: bfloat16 [1024, 2048], P('tp'), may hold values from -0.1875 to 0.1875
- post_gain: float32 [2048], replicated, may hold values from 0.1 to 1.9
- moe_in: bfloat16 [1024, 2048], P('ep'), may hold values from -6 to 6
- routes: int32 [1024, 2], P('ep'), may hold values from 0 to 7, all different within a row; in each aligned block of 128 rows (0 to 127, 128 to 255, ...) at most 48 rows name the same one
- route_logits: float32 [1024, 2], P('ep'), may hold values from -6 to 6
- pre_gain: float32 [2048], replicated, may hold values from 0.1 to 1.9
- w_gate: bfloat16 [8, 2048, 4096], P('ep', None, 'tp'), may hold values from -0.125 to 0.125
- w_up: bfloat16 [8, 2048, 4096], P('ep', None, 'tp'), may hold values from -0.125 to 0.125
- w_down: bfloat16 [8, 4096, 2048], P('ep', 'tp'), may hold values from -0.125 to 0.125
Outputs:
- attn_out: bfloat16 [4096, 2048], P(('ep', 'tp'))
- moe_out: bfloat16 [1024, 2048], P('ep', 'tp')
Inputs may be any that keep to these rules, and one draw needn't show every extreme that they name: `routes`: each row names 2 different experts. Among the rows of one index of ep no expert is named by more than 48 rows, a bound that some block reaches of them.
All inputs are finite; a program needn't handle non-finite values.
Results may differ from a plain program's by a relative error of at most 0.018.
Values may be sent and summed in bfloat16 or wider, within the bound.
A program may use at most 64 MiB of HBM per device.

v0:
```python
import jax
import jax.numpy as jnp
from jax import lax
from jax.sharding import PartitionSpec as P

GRID_W = 128
EPSILON = 1e-06
ROPE_BASE = 10000.0


def head_norm(values, gain):
    return values * lax.rsqrt(jnp.mean(values * values, axis=-1, keepdims=True) + EPSILON) * gain


def rotate_half(values, angles):
    quarter = angles.shape[-1]
    first_part = values[..., :quarter]
    second_part = values[..., quarter:]
    cosine = jnp.cos(angles)[:, None, :]
    sine_part = jnp.sin(angles)[:, None, :]
    return jnp.concatenate(
        [
            first_part * cosine - second_part * sine_part,
            second_part * cosine + first_part * sine_part,
        ],
        axis=-1,
    )


def grid_rotary(values, offset):
    row_count = values.shape[0]
    head_width = values.shape[-1]
    quarter = head_width // 4
    half_width = head_width // 2
    position = offset + jnp.arange(row_count, dtype=jnp.int32)
    grid_row = (position // GRID_W).astype(jnp.float32)
    grid_col = (position % GRID_W).astype(jnp.float32)
    inverse = ROPE_BASE ** (-jnp.arange(quarter, dtype=jnp.float32) / quarter)
    return jnp.concatenate(
        [
            rotate_half(values[..., :half_width], grid_row[:, None] * inverse[None, :]),
            rotate_half(values[..., half_width:], grid_col[:, None] * inverse[None, :]),
        ],
        axis=-1,
    )


def slot_table(route_rows, expert_count, capacity):
    token_count, top_count = route_rows.shape
    flat_routes = route_rows.reshape(-1)
    one_hot = (flat_routes[:, None] == jnp.arange(expert_count, dtype=jnp.int32)[None, :]).astype(
        jnp.int32
    )
    ranked = jnp.sum((jnp.cumsum(one_hot, axis=0) - 1) * one_hot, axis=1)
    placed = flat_routes * capacity + ranked
    slot_owner = jnp.full((expert_count * capacity,), token_count * top_count, dtype=jnp.int32)
    slot_owner = slot_owner.at[placed].set(jnp.arange(token_count * top_count, dtype=jnp.int32))
    return (slot_owner, placed)


def mixer_half(q_in, k_in, v_in, q_gain, k_gain, w_out, post_gain):
    head_size = q_gain.shape[0]
    row_count = q_in.shape[0]
    local_heads = q_in.shape[1] // head_size
    kv_count = k_in.shape[1] // head_size
    tp_count = lax.axis_size("tp")
    repeat = local_heads * tp_count // kv_count
    offset = lax.axis_index("ep") * row_count
    queries = head_norm(q_in.astype(jnp.float32).reshape(row_count, local_heads, head_size), q_gain)
    queries = grid_rotary(queries, offset).astype(jnp.bfloat16)
    query_rows = jnp.transpose(queries, (1, 0, 2)).reshape(local_heads * row_count, head_size)
    kv_index = lax.axis_index("tp") * local_heads // repeat
    own_keys = lax.dynamic_slice_in_dim(k_in, kv_index * head_size, head_size, 1)
    own_values = lax.dynamic_slice_in_dim(v_in, kv_index * head_size, head_size, 1)
    own_keys = head_norm(own_keys.astype(jnp.float32)[:, None, :], k_gain)
    own_keys = grid_rotary(own_keys, offset)[:, 0, :].astype(jnp.bfloat16)
    paired = jnp.concatenate([own_keys, own_values], axis=1)
    scale_factor = head_size ** (-0.5)

    def attend_block(running, key_block):
        block_keys = key_block[:, :head_size]
        block_values = key_block[:, head_size:]
        scores = (
            jnp.einsum("qd,kd->qk", query_rows, block_keys, preferred_element_type=jnp.float32)
            * scale_factor
        )
        weights = jnp.exp(scores)
        numer = running[0] + jnp.dot(
            weights.astype(jnp.bfloat16), block_values, preferred_element_type=jnp.float32
        )
        return (numer, running[1] + jnp.sum(weights, axis=1))

    zero_init = (
        jnp.zeros((local_heads * row_count, head_size), jnp.float32),
        jnp.zeros((local_heads * row_count,), jnp.float32),
    )
    running = zero_init
    gathered_piece = lax.all_gather(paired, "ep", axis=0, tiled=True)
    piece_rows = gathered_piece.shape[0]
    blocks = gathered_piece.reshape(piece_rows // 512, 512, gathered_piece.shape[1])

    def scan_block(partial_value, key_block):
        return (attend_block(partial_value, key_block), None)

    running, unused = lax.scan(scan_block, running, blocks)
    numer, denom = running
    head_out = (numer / denom[:, None]).astype(jnp.bfloat16)
    head_out = jnp.transpose(head_out.reshape(local_heads, row_count, head_size), (1, 0, 2))
    head_out = head_out.reshape(row_count, local_heads * head_size)
    mixed = lax.psum_scatter(
        jnp.dot(head_out, w_out, preferred_element_type=jnp.float32).astype(jnp.bfloat16),
        "tp",
        scatter_dimension=0,
        tiled=True,
    ).astype(jnp.float32)
    return head_norm(mixed, post_gain).astype(jnp.bfloat16)


def experts_half(moe_in, routes, route_logits, pre_gain, w_gate, w_up, w_down):
    token_count, top_count = routes.shape
    model_width = moe_in.shape[1]
    expert_count = lax.axis_size("ep")
    capacity = max(2, 3 * top_count * token_count // (2 * expert_count))
    tp_count = lax.axis_size("tp")
    slice_width = model_width // tp_count
    normed = head_norm(moe_in.astype(jnp.float32), pre_gain).astype(jnp.bfloat16)
    slot_owner, placed = slot_table(routes, expert_count, capacity)
    padded = jnp.concatenate([normed, jnp.zeros((1, model_width), jnp.bfloat16)], axis=0)
    outgoing = padded[slot_owner // top_count].reshape(expert_count, capacity, model_width)
    arrived = lax.all_to_all(outgoing, "ep", split_axis=0, concat_axis=0, tiled=True)
    arrived = arrived.reshape(expert_count * capacity, model_width)
    gate_pre = jnp.dot(arrived, w_gate[0], preferred_element_type=jnp.float32)
    up_pre = jnp.dot(arrived, w_up[0], preferred_element_type=jnp.float32)
    hidden = (jax.nn.silu(gate_pre) * up_pre).astype(jnp.bfloat16)
    partial_out = jnp.dot(hidden, w_down[0], preferred_element_type=jnp.float32)
    partial_out = partial_out.reshape(expert_count, capacity, model_width)
    summed = lax.psum_scatter(
        partial_out.astype(jnp.bfloat16), "tp", scatter_dimension=2, tiled=True
    )
    returned = lax.all_to_all(summed, "ep", split_axis=0, concat_axis=0, tiled=True)
    returned = returned.reshape(expert_count * capacity, slice_width)
    copies = returned[placed].reshape(token_count, top_count, slice_width).astype(jnp.float32)
    route_weight = jax.nn.softmax(route_logits, axis=-1)
    return jnp.sum(route_weight[..., None] * copies, axis=1).astype(jnp.bfloat16)


def per_device(
    q_in,
    k_in,
    v_in,
    q_gain,
    k_gain,
    w_out,
    post_gain,
    moe_in,
    routes,
    route_logits,
    pre_gain,
    w_gate,
    w_up,
    w_down,
):
    attn_out = mixer_half(q_in, k_in, v_in, q_gain, k_gain, w_out, post_gain)
    moe_out = experts_half(moe_in, routes, route_logits, pre_gain, w_gate, w_up, w_down)
    return (attn_out, moe_out)


def solution(mesh):
    return jax.shard_map(
        per_device,
        mesh=mesh,
        in_specs=(
            P("ep", "tp"),
            P("ep", None),
            P("ep", None),
            P(),
            P(),
            P("tp", None),
            P(),
            P("ep", None),
            P("ep", None),
            P("ep", None),
            P(),
            P("ep", None, "tp"),
            P("ep", None, "tp"),
            P("ep", "tp", None),
        ),
        out_specs=(P(("ep", "tp"), None), P("ep", "tp")),
        check_vma=False,
    )
```

profile of v0, /device:TPU:0, one launch (start us, length us, event | category | flops | bytes accessed | tf_op | source)
XLA Modules:
  0.0 186.0 jit_solution(11214696343545034479)
XLA Ops:
  11.1 1.4 scatter_custom_fusion
  12.5 1.2 fusion.22
  13.7 1.2 fusion.24
  15.0 3.1 %gather_fusion = bf16[384,2048]{1,0:T(8,128)(2,1)} fusion(bf16[129,2048]{1,0:T(8,128)(2,1)S(1)} %concatenate.17, s32[1024]{0:T(1024)S(1)} %pad_clamp_fusion.1), kind=kCustom, calls=%fused_computation | custom fusion | bytes 3147264 | tf_op jit(solution)/shard_map/gather | solution.py:129
  18.2 7.4 %all-to-all-start = ((bf16[8,48,2048]{2,1,0:T(8,128)(2,1)}), bf16[8,48,2048]{2,1,0:T(8,128)(2,1)}, u32[]{:S(2)}, u32[]{:S(2)}) async-start(bf16[8,48,2048]{2,1,0:T(8,128)(2,1)} %bitcast.13), calls=%async_computation.1 | async-start | bytes 3145728 | tf_op jit(solution)/shard_map/all_to_all | solution.py:130
  28.4 50.5 %all-gather.2.cloned.1.call-done = bf16[4096,128]{0,1:T(8,128)(2,1)} async-done(((bf16[512,128]{0,1:T(8,128)(2,1)}), bf16[4096,128]{0,1:T(8,128)(2,1)}) %all-gather.2.cloned.1.call-update) | async-done | bytes 1048592 | tf_op jit(solution)/shard_map/all_gather | solution.py:98
  78.9 1.6 copy.42
  80.6 4.6 %fusion.12 = f32[384,1024]{1,0:T(8,128)S(1)} fusion(bf16[384,2048]{1,0:T(8,128)(2,1)} %bitcast.14, bf16[1,2048,1024]{2,1,0:T(8,128)(2,1)} %param.27), kind=kOutput, calls=%fused_computation.18 | convolution fusion | flops 1610612736 | bytes 7340032 | tf_op jit(solution)/shard_map/dot_general | solution.py:132
  85.2 3.5 %multiply_convert_fusion = bf16[384,1024]{1,0:T(8,128)(2,1)S(1)} fusion(f32[384,1024]{1,0:T(8,128)S(1)} %fusion.12, bf16[384,2048]{1,0:T(8,128)(2,1)} %bitcast.14, bf16[1,2048,1024]{2,1,0:T(8,128)(2,1)S(1)} %copy-done.8), kind=kOutput, calls=%fused_computation.22 | convolution fusion | flops 1612972032 | bytes 8126464 | tf_op jit(solution)/shard_map/dot_general | solution.py:133
  88.8 3.0 %fusion.14 = bf16[8,48,2048]{2,1,0:T(8,128)(2,1)} fusion(bf16[8,48,1024]{2,1,0:T(8,128)(2,1)S(1)} %bitcast.62, bf16[1,1024,2048]{2,1,0:T(8,128)(2,1)S(1)} %copy-done.9), kind=kOutput, calls=%fused_computation.21 | convolution fusion | flops 1611399168 | bytes 6553600 | tf_op jit(solution)/shard_map/dot_general | solution.py:135
  91.8 46.4 %while.13 = (s32[]{:T(128)}, f32[2048,64]{0,1:T(8,128)S(1)}, f32[2048]{0:T(1024)S(1)}, bf16[8,512,128]{2,1,0:T(8,128)(2,1)S(1)}, bf16[2048,64]{1,0:T(8,128)(2,1)S(1)}, /*index=5*/s32[]{:T(128)}, s32[]{:T(128)}) while((s32[]{:T(128)}, f32[2048,64]{0,1:T(8,128)S(1)}, f32[2048]{0:T(1024)S(1)}, bf16[8,512,128]{2,1,0:T(8,128)(2,1)S(1)}, ...), condition=%wide.region_4.5_spmd.clone, body=%wide.region_2.4_spmd.clone.sunk | while | flops 272893952 | bytes 10256476 | solution.py:105
  91.9 2.7 %fusion.72 = (f32[2048]{0:T(1024)S(1)}, f32[512,2048]{1,0:T(8,128)}) fusion(bf16[2048,64]{1,0:T(8,128)(2,1)S(1)} %get-tuple-element.147, bf16[512,128]{1,0:T(8,128)(2,1)S(1)} %dynamic-slice_bitcast_fusion.2), kind=kOutput, calls=%fused_computation.4.clone.1 | convolution fusion | flops 136312832 | bytes 4595712 | tf_op jit(solution)/shard_map/while/body/eval_jaxpr/qd,kd->qk/dot_general | solution.py:84
  94.5 3.1 %convolution_add_fusion.2 = f32[2048,64]{0,1:T(8,128)S(1)} fusion(f32[512,2048]{1,0:T(8,128)} %get-tuple-element.127, f32[2048,64]{0,1:T(8,128)S(1)} %get-tuple-element.137, pred[]{:T(512)S(6)} %compare.19, bf16[512,128]{1,0:T(8,128)(2,1)S(1)} %dynamic-slice_bitcast_fusion.2), kind=kOutput, calls=%fused_computation.6.clone.1 | convolution fusion | flops 136577024 | bytes 5373953 | tf_op jit(solution)/shard_map/while/body/eval_jaxpr/dot_general | solution.py:88
  97.7 2.7 %fusion.72 = (f32[2048]{0:T(1024)S(1)}, f32[512,2048]{1,0:T(8,128)}) fusion(bf16[2048,64]{1,0:T(8,128)(2,1)S(1)} %get-tuple-element.147, bf16[512,128]{1,0:T(8,128)(2,1)S(1)} %dynamic-slice_bitcast_fusion.2), kind=kOutput, calls=%fused_computation.4.clone.1 | convolution fusion | flops 136312832 | bytes 4595712 | tf_op jit(solution)/shard_map/while/body/eval_jaxpr/qd,kd->qk/dot_general | solution.py:84
  100.3 3.2 %convolution_add_fusion.2 = f32[2048,64]{0,1:T(8,128)S(1)} fusion(f32[512,2048]{1,0:T(8,128)} %get-tuple-element.127, f32[2048,64]{0,1:T(8,128)S(1)} %get-tuple-element.137, pred[]{:T(512)S(6)} %compare.19, bf16[512,128]{1,0:T(8,128)(2,1)S(1)} %dynamic-slice_bitcast_fusion.2), kind=kOutput, calls=%fused_computation.6.clone.1 | convolution fusion | flops 136577024 | bytes 5373953 | tf_op jit(solution)/shard_map/while/body/eval_jaxpr/dot_general | solution.py:88
  103.5 2.7 %fusion.72 = (f32[2048]{0:T(1024)S(1)}, f32[512,2048]{1,0:T(8,128)}) fusion(bf16[2048,64]{1,0:T(8,128)(2,1)S(1)} %get-tuple-element.147, bf16[512,128]{1,0:T(8,128)(2,1)S(1)} %dynamic-slice_bitcast_fusion.2), kind=kOutput, calls=%fused_computation.4.clone.1 | convolution fusion | flops 136312832 | bytes 4595712 | tf_op jit(solution)/shard_map/while/body/eval_jaxpr/qd,kd->qk/dot_general | solution.py:84
  106.2 3.1 %convolution_add_fusion.2 = f32[2048,64]{0,1:T(8,128)S(1)} fusion(f32[512,2048]{1,0:T(8,128)} %get-tuple-element.127, f32[2048,64]{0,1:T(8,128)S(1)} %get-tuple-element.137, pred[]{:T(512)S(6)} %compare.19, bf16[512,128]{1,0:T(8,128)(2,1)S(1)} %dynamic-slice_bitcast_fusion.2), kind=kOutput, calls=%fused_computation.6.clone.1 | convolution fusion | flops 136577024 | bytes 5373953 | tf_op jit(solution)/shard_map/while/body/eval_jaxpr/dot_general | solution.py:88
  109.3 2.7 %fusion.72 = (f32[2048]{0:T(1024)S(1)}, f32[512,2048]{1,0:T(8,128)}) fusion(bf16[2048,64]{1,0:T(8,128)(2,1)S(1)} %get-tuple-element.147, bf16[512,128]{1,0:T(8,128)(2,1)S(1)} %dynamic-slice_bitcast_fusion.2), kind=kOutput, calls=%fused_computation.4.clone.1 | convolution fusion | flops 136312832 | bytes 4595712 | tf_op jit(solution)/shard_map/while/body/eval_jaxpr/qd,kd->qk/dot_general | solution.py:84
  112.0 3.1 %convolution_add_fusion.2 = f32[2048,64]{0,1:T(8,128)S(1)} fusion(f32[512,2048]{1,0:T(8,128)} %get-tuple-element.127, f32[2048,64]{0,1:T(8,128)S(1)} %get-tuple-element.137, pred[]{:T(512)S(6)} %compare.19, bf16[512,128]{1,0:T(8,128)(2,1)S(1)} %dynamic-slice_bitcast_fusion.2), kind=kOutput, calls=%fused_computation.6.clone.1 | convolution fusion | flops 136577024 | bytes 5373953 | tf_op jit(solution)/shard_map/while/body/eval_jaxpr/dot_general | solution.py:88
  115.1 2.7 %fusion.72 = (f32[2048]{0:T(1024)S(1)}, f32[512,2048]{1,0:T(8,128)}) fusion(bf16[2048,64]{1,0:T(8,128)(2,1)S(1)} %get-tuple-element.147, bf16[512,128]{1,0:T(8,128)(2,1)S(1)} %dynamic-slice_bitcast_fusion.2), kind=kOutput, calls=%fused_computation.4.clone.1 | convolution fusion | flops 136312832 | bytes 4595712 | tf_op jit(solution)/shard_map/while/body/eval_jaxpr/qd,kd->qk/dot_general | solution.py:84
  117.8 3.1 %convolution_add_fusion.2 = f32[2048,64]{0,1:T(8,128)S(1)} fusion(f32[512,2048]{1,0:T(8,128)} %get-tuple-element.127, f32[2048,64]{0,1:T(8,128)S(1)} %get-tuple-element.137, pred[]{:T(512)S(6)} %compare.19, bf16[512,128]{1,0:T(8,128)(2,1)S(1)} %dynamic-slice_bitcast_fusion.2), kind=kOutput, calls=%fused_computation.6.clone.1 | convolution fusion | flops 136577024 | bytes 5373953 | tf_op jit(solution)/shard_map/while/body/eval_jaxpr/dot_general | solution.py:88
  120.9 2.7 %fusion.72 = (f32[2048]{0:T(1024)S(1)}, f32[512,2048]{1,0:T(8,128)}) fusion(bf16[2048,64]{1,0:T(8,128)(2,1)S(1)} %get-tuple-element.147, bf16[512,128]{1,0:T(8,128)(2,1)S(1)} %dynamic-slice_bitcast_fusion.2), kind=kOutput, calls=%fused_computation.4.clone.1 | convolution fusion | flops 136312832 | bytes 4595712 | tf_op jit(solution)/shard_map/while/body/eval_jaxpr/qd,kd->qk/dot_general | solution.py:84
  123.6 3.1 %convolution_add_fusion.2 = f32[2048,64]{0,1:T(8,128)S(1)} fusion(f32[512,2048]{1,0:T(8,128)} %get-tuple-element.127, f32[2048,64]{0,1:T(8,128)S(1)} %get-tuple-element.137, pred[]{:T(512)S(6)} %compare.19, bf16[512,128]{1,0:T(8,128)(2,1)S(1)} %dynamic-slice_bitcast_fusion.2), kind=kOutput, calls=%fused_computation.6.clone.1 | convolution fusion | flops 136577024 | bytes 5373953 | tf_op jit(solution)/shard_map/while/body/eval_jaxpr/dot_general | solution.py:88
  126.7 2.7 %fusion.72 = (f32[2048]{0:T(1024)S(1)}, f32[512,2048]{1,0:T(8,128)}) fusion(bf16[2048,64]{1,0:T(8,128)(2,1)S(1)} %get-tuple-element.147, bf16[512,128]{1,0:T(8,128)(2,1)S(1)} %dynamic-slice_bitcast_fusion.2), kind=kOutput, calls=%fused_computation.4.clone.1 | convolution fusion | flops 136312832 | bytes 4595712 | tf_op jit(solution)/shard_map/while/body/eval_jaxpr/qd,kd->qk/dot_general | solution.py:84
  129.4 3.1 %convolution_add_fusion.2 = f32[2048,64]{0,1:T(8,128)S(1)} fusion(f32[512,2048]{1,0:T(8,128)} %get-tuple-element.127, f32[2048,64]{0,1:T(8,128)S(1)} %get-tuple-element.137, pred[]{:T(512)S(6)} %compare.19, bf16[512,128]{1,0:T(8,128)(2,1)S(1)} %dynamic-slice_bitcast_fusion.2), kind=kOutput, calls=%fused_computation.6.clone.1 | convolution fusion | flops 136577024 | bytes 5373953 | tf_op jit(solution)/shard_map/while/body/eval_jaxpr/dot_general | solution.py:88
  132.5 2.7 %fusion.72 = (f32[2048]{0:T(1024)S(1)}, f32[512,2048]{1,0:T(8,128)}) fusion(bf16[2048,64]{1,0:T(8,128)(2,1)S(1)} %get-tuple-element.147, bf16[512,128]{1,0:T(8,128)(2,1)S(1)} %dynamic-slice_bitcast_fusion.2), kind=kOutput, calls=%fused_computation.4.clone.1 | convolution fusion | flops 136312832 | bytes 4595712 | tf_op jit(solution)/shard_map/while/body/eval_jaxpr/qd,kd->qk/dot_general | solution.py:84
  135.2 3.1 %convolution_add_fusion.2 = f32[2048,64]{0,1:T(8,128)S(1)} fusion(f32[512,2048]{1,0:T(8,128)} %get-tuple-element.127, f32[2048,64]{0,1:T(8,128)S(1)} %get-tuple-element.137, pred[]{:T(512)S(6)} %compare.19, bf16[512,128]{1,0:T(8,128)(2,1)S(1)} %dynamic-slice_bitcast_fusion.2), kind=kOutput, calls=%fused_computation.6.clone.1 | convolution fusion | flops 136577024 | bytes 5373953 | tf_op jit(solution)/shard_map/while/body/eval_jaxpr/dot_general | solution.py:88
  138.6 2.1 %convolution_convert_fusion = bf16[512,2048]{1,0:T(8,128)(2,1)} fusion(bf16[512,256]{0,1:T(8,128)(2,1)S(1)} %bitcast.57, bf16[256,2048]{1,0:T(8,128)(2,1)S(1)} %copy-done), kind=kOutput, calls=%fused_computation.20 | convolution fusion | flops 537919488 | bytes 3407872 | tf_op jit(solution)/shard_map/dot_general | solution.py:111
  141.6 5.0 %all-to-all-start.1 = ((bf16[8,48,512]{2,1,0:T(8,128)(2,1)}), bf16[8,48,512]{2,1,0:T(8,128)(2,1)S(1)}, u32[]{:S(2)}, u32[]{:S(2)}) async-start(bf16[8,48,512]{2,1,0:T(8,128)(2,1)} %reduce-scatter.5.cloned.1.call-done), calls=%async_computation.3 | async-start | bytes 786432 | tf_op jit(solution)/shard_map/all_to_all | solution.py:140
  146.6 25.8 %reduce-scatter.3.cloned.1.call-done = bf16[128,2048]{1,0:T(8,128)(2,1)} async-done(((bf16[512,2048]{1,0:T(8,128)(2,1)}), bf16[128,2048]{1,0:T(8,128)(2,1)}) %reduce-scatter.3.cloned.1.call-update) | async-done | bytes 524304 | tf_op jit(solution)/shard_map/reduce_scatter | solution.py:110
  173.7 2.0 %fusion.21 = bf16[128,2048]{1,0:T(8,128)(2,1)} fusion(bf16[128,2048]{1,0:T(8,128)(2,1)} %reduce-scatter.3.cloned.1.call-done, f32[2048]{0:T(1024)S(1)} %copy-done.5, f32[128]{0:T(128)S(1)} %add_rsqrt_fusion.3), kind=kLoop, calls=%fused_computation.29 | loop fusion | flops 1048576 | bytes 1057280 | tf_op jit(solution)/shard_map/convert_element_type | solution.py:116
  177.2 1.4 multiply_reduce_fusion
  (96 shorter events, 9.8 us)
Async XLA Ops:
  8.0 130.6 %copy-start = (bf16[256,2048]{1,0:T(8,128)(2,1)S(1)}, bf16[256,2048]{1,0:T(8,128)(2,1)}, u32[]{:S(2)}) copy-start(bf16[256,2048]{1,0:T(8,128)(2,1)} %param.21) | copy-start | bytes 3145732
  18.1 7.5 %copy-start.2 = (bf16[512,256]{1,0:T(8,128)(2,1)S(1)}, bf16[512,256]{1,0:T(8,128)(2,1)}, u32[]{:S(2)}) copy-start(bf16[512,256]{1,0:T(8,128)(2,1)} %param.18) | copy-start | bytes 786436
  18.2 7.5 %copy-start.3 = (bf16[512,256]{1,0:T(8,128)(2,1)S(1)}, bf16[512,256]{1,0:T(8,128)(2,1)}, u32[]{:S(2)}) copy-start(bf16[512,256]{1,0:T(8,128)(2,1)} %param.17) | copy-start | bytes 786436
  18.2 8.0 %copy-start.6 = (f32[64]{0:T(128)S(1)}, f32[64]{0:T(128)}, u32[]{:S(2)}) copy-start(f32[64]{0:T(128)} %param.20) | copy-start | bytes 772
  18.2 9.2 %copy-start.1 = (bf16[512,256]{1,0:T(8,128)(2,1)S(1)}, bf16[512,256]{1,0:T(8,128)(2,1)}, u32[]{:S(2)}) copy-start(bf16[512,256]{1,0:T(8,128)(2,1)} %param.16) | copy-start | bytes 786436
  18.2 62.4 %all-to-all-start = ((bf16[8,48,2048]{2,1,0:T(8,128)(2,1)}), bf16[8,48,2048]{2,1,0:T(8,128)(2,1)}, u32[]{:S(2)}, u32[]{:S(2)}) async-start(bf16[8,48,2048]{2,1,0:T(8,128)(2,1)} %bitcast.13), calls=%async_computation.1 | async-start | bytes 3145728 | tf_op jit(solution)/shard_map/all_to_all | solution.py:130
  25.6 2.3 %copy-start.7 = (f32[64]{0:T(128)S(1)}, f32[64]{0:T(128)}, u32[]{:S(2)}) copy-start(f32[64]{0:T(128)} %param.19) | copy-start | bytes 772
  25.6 53.3 %all-gather.2.cloned.1.call-start = ((), (), s32[]{:S(2)}) async-start(), calls=%async_computation.4 | async-start | bytes 1179648 | tf_op jit(solution)/shard_map/all_gather | solution.py:98
  27.2 114.3 %reduce-scatter.5.cloned.1.call-start = ((), (), s32[]{:S(2)}) async-start(), calls=%async_computation.6 | async-start | bytes 1966080 | tf_op jit(solution)/shard_map/reduce_scatter | solution.py:137
  80.6 4.6 %copy-start.8 = (bf16[1,2048,1024]{2,1,0:T(8,128)(2,1)S(1)}, bf16[1,2048,1024]{2,1,0:T(8,128)(2,1)}, u32[]{:S(2)}) copy-start(bf16[1,2048,1024]{2,1,0:T(8,128)(2,1)} %param.28) | copy-start | bytes 12582916
  85.2 3.6 %copy-start.9 = (bf16[1,1024,2048]{2,1,0:T(8,128)(2,1)S(1)}, bf16[1,1024,2048]{2,1,0:T(8,128)(2,1)}, u32[]{:S(2)}) copy-start(bf16[1,1024,2048]{2,1,0:T(8,128)(2,1)} %param.29) | copy-start | bytes 12582916
  91.8 80.6 %reduce-scatter.3.cloned.1.call-start = ((), (), s32[]{:S(2)}) async-start(), calls=%async_computation.5 | async-start | bytes 2621440 | tf_op jit(solution)/shard_map/reduce_scatter | solution.py:110
  140.7 0.7 copy-start.4
  140.7 33.0 %copy-start.5 = (f32[2048]{0:T(1024)S(1)}, f32[2048]{0:T(1024)}, u32[]{:S(2)}) copy-start(f32[2048]{0:T(1024)} %param.22) | copy-start | bytes 24580
  141.6 34.1 %all-to-all-start.1 = ((bf16[8,48,512]{2,1,0:T(8,128)(2,1)}), bf16[8,48,512]{2,1,0:T(8,128)(2,1)S(1)}, u32[]{:S(2)}, u32[]{:S(2)}) async-start(bf16[8,48,512]{2,1,0:T(8,128)(2,1)} %reduce-scatter.5.cloned.1.call-done), calls=%async_computation.3 | async-start | bytes 786432 | tf_op jit(solution)/shard_map/all_to_all | solution.py:140
Sparse Core Ops, SparseCore 0:
  29.0 49.8 all-gather.1
Sparse Core Ops, SparseCore 1:
  91.9 28.3 reduce-scatter.4
  140.8 31.6 reduce-scatter.2
where the time goes:
time: 187 us; the launch traced here: 186 us
  waiting for transfers between devices  76.5 us (41%)
  matrix products  59.2 us (32%)
  between operations  15.9 us (9%)
  starting transfers between devices  12.5 us (7%)
  local copies, waits for them, and re-layouts  11.2 us (6%)
  other arithmetic  10.4 us (6%)
    all_gather x1, waiting for transfers between devices, mixer_half(): gathered_piece = lax.all_gather(paired, 'ep', axis=0, tiled=True)  50.5 us
    reduce_scatter x1, waiting for transfers between devices, mixer_half(): lax.psum_scatter(jnp.dot(head_out, w_out, preferred_element_type=jnp.floa...  25.8 us
    dot_general x8, matrix products, attend_block(): jnp.dot(weights.astype(jnp.bfloat16), block_values, preferred_element_typ...  24.7 us
    dot_general x8, matrix products, attend_block(): jnp.einsum('qd,kd->qk', query_rows, block_keys, preferred_element_type=jn...  21.2 us
    all_to_all x1, starting transfers between devices, experts_half(): lax.all_to_all(outgoing, 'ep', split_axis=0, concat_axis=0, tiled=True)  7.42 us
    all_to_all x1, starting transfers between devices, experts_half(): lax.all_to_all(summed, 'ep', split_axis=0, concat_axis=0, tiled=True)  4.98 us
    dot_general x1, matrix products, experts_half(): gate_pre = jnp.dot(arrived, w_gate[0], preferred_element_type=jnp.float32)  4.59 us
    unnamed x26, local copies, waits for them, and re-layouts  3.79 us
  transfers between devices with their start and end apart: 5, of which 2 were waited for; matrix products, arithmetic and copies ran while one was open for 30% of the time, Pallas kernels for 0%

commit v1 on v0

--- a/solution.py
+++ b/solution.py
@@ -6,6 +6,28 @@
 GRID_W = 128
 EPSILON = 1e-06
 ROPE_BASE = 10000.0
+
+
+def in_order(pieces, dim):
+    pieces = jnp.moveaxis(pieces, 0, dim)
+    dims = pieces.shape
+    return pieces.reshape(*dims[:dim], dims[dim] * dims[dim + 1], *dims[dim + 2 :])
+
+
+def ring_gather(x, axis, dim):
+    size = lax.axis_size(axis)
+    pairs = [(i, (i + 1) % size) for i in range(size)]
+    back = [(b, a) for a, b in pairs]
+    lower, upper = ([], [])
+    for step in range(size - 1):
+        if step % 2 == 0:
+            lower.append(lax.ppermute(lower[-1] if lower else x, axis, pairs))
+        else:
+            upper.append(lax.ppermute(upper[-1] if upper else x, axis, back))
+    tiles = jnp.stack([*lower[::-1], x, *upper])
+    shift = lax.axis_index(axis) - len(lower)
+    tiles = tiles[(jnp.arange(size) - shift) % size]
+    return in_order(tiles, dim)
 
 
 def head_norm(values, gain):
@@ -95,7 +117,7 @@
         jnp.zeros((local_heads * row_count,), jnp.float32),
     )
     running = zero_init
-    gathered_piece = lax.all_gather(paired, "ep", axis=0, tiled=True)
+    gathered_piece = ring_gather(paired, "ep", 0)
     piece_rows = gathered_piece.shape[0]
     blocks = gathered_piece.reshape(piece_rows // 512, 512, gathered_piece.shape[1])
 

time: 187 us -> 226 us (1.21)
  waiting for transfers between devices: 76.5 us -> 97.5 us
  starting transfers between devices: 12.5 us -> 27.8 us
  local copies, waits for them, and re-layouts: 11.2 us -> 17.3 us
    all_gather x1 -> x0, waiting for transfers between devices: 50.5 us -> none  [mixer_half(): gathered_piece = lax.all_gather(paired, 'ep', axis=0, tiled=True)]
    ppermute x0 -> x7, waiting for transfers between devices: none -> 36.1 us  [the longest x4 36.1 us: ring_gather(): lower.append(lax.ppermute(lower[-1] if lower else x, axis, pairs))]
    reduce_scatter x1, waiting for transfers between devices: 0.03 us -> 29.4 us  [experts_half(): lax.psum_scatter(partial_out.astype(jnp.bfloat16), 'tp', scatter_dimensio...]
    ppermute x0 -> x7, starting transfers between devices: none -> 17.6 us  [the longest x3 12.6 us: ring_gather(): upper.append(lax.ppermute(upper[-1] if upper else x, axis, back))]
    all_to_all x1, waiting for transfers between devices: 0.01 us -> 9.51 us  [experts_half(): lax.all_to_all(summed, 'ep', split_axis=0, concat_axis=0, tiled=True)]
    reduce_scatter x1, waiting for transfers between devices: 25.8 us -> 22.4 us  [mixer_half(): lax.psum_scatter(jnp.dot(head_out, w_out, preferred_element_type=jnp.floa...]
    all_to_all x1, starting transfers between devices: 7.42 us -> 4.42 us  [experts_half(): lax.all_to_all(outgoing, 'ep', split_axis=0, concat_axis=0, tiled=True)]
    unnamed x26 -> x29, local copies, waits for them, and re-layouts: 3.79 us -> 5.38 us
  transfers between devices with their start and end apart: 5 -> 11, of which waited for: 2 -> 6; matrix products, arithmetic and copies ran while one was open for 30% -> 35% of each run, Pallas kernels for 0% -> 0%
where the time goes in v1:
time: 226 us
  waiting for transfers between devices  97.5 us (43%)
  matrix products  59.1 us (26%)
  starting transfers between devices  27.8 us (12%)
  local copies, waits for them, and re-layouts  17.3 us (8%)
  between operations  14.5 us (6%)
  other arithmetic  8.98 us (4%)
    ppermute x4, waiting for transfers between devices, ring_gather(): lower.append(lax.ppermute(lower[-1] if lower else x, axis, pairs))  36.1 us
    reduce_scatter x1, waiting for transfers between devices, experts_half(): lax.psum_scatter(partial_out.astype(jnp.bfloat16), 'tp', scatter_dimensio...  29.4 us
    dot_general x8, matrix products, attend_block(): jnp.dot(weights.astype(jnp.bfloat16), block_values, preferred_element_typ...  24.6 us
    reduce_scatter x1, waiting for transfers between devices, mixer_half(): lax.psum_scatter(jnp.dot(head_out, w_out, preferred_element_type=jnp.floa...  22.4 us
    dot_general x8, matrix products, attend_block(): jnp.einsum('qd,kd->qk', query_rows, block_keys, preferred_element_type=jn...  21.3 us
    ppermute x3, starting transfers between devices, ring_gather(): upper.append(lax.ppermute(upper[-1] if upper else x, axis, back))  12.6 us
    all_to_all x1, waiting for transfers between devices, experts_half(): lax.all_to_all(summed, 'ep', split_axis=0, concat_axis=0, tiled=True)  9.51 us
    all_to_all x1, starting transfers between devices, experts_half(): lax.all_to_all(summed, 'ep', split_axis=0, concat_axis=0, tiled=True)  5.51 us
  transfers between devices with their start and end apart: 11, of which 6 were waited for; matrix products, arithmetic and copies ran while one was open for 35% of the time, Pallas kernels for 0%

profile of v1, /device:TPU:0, one launch (start us, length us, event | category | flops | bytes accessed | tf_op | source)
XLA Modules:
  0.0 225.5 jit_solution(9066628744527531024)
XLA Ops:
  9.8 3.0 %collective-permute-start = (bf16[512,128]{0,1:T(8,128)(2,1)S(1)}, bf16[512,128]{0,1:T(8,128)(2,1)S(1)}, u32[]{:S(2)}, u32[]{:S(2)}) collective-permute-start(bf16[512,128]{0,1:T(8,128)(2,1)S(1)} %pad_maximum_fusion), channel_id=1, source_target_pairs={{0,4},{4,8},{8,12},{12,16},{16,20},{20,24},{24,28},{28,0},{1,5},{5... | collective-permute-start | bytes 393224 | tf_op jit(solution)/shard_map/ppermute | solution.py:24
  12.9 3.1 %collective-permute-start.4 = (bf16[512,128]{0,1:T(8,128)(2,1)S(1)}, bf16[512,128]{0,1:T(8,128)(2,1)S(1)}, u32[]{:S(2)}, u32[]{:S(2)}) collective-permute-start(bf16[512,128]{0,1:T(8,128)(2,1)S(1)} %pad_maximum_fusion), channel_id=1, source_target_pairs={{4,0},{8,4},{12,8},{16,12},{20,16},{24,20},{28,24},{0,28},{5,1},{9... | collective-permute-start | bytes 393224 | tf_op jit(solution)/shard_map/ppermute | solution.py:26
  20.8 3.1 %gather_fusion.1 = bf16[384,2048]{1,0:T(8,128)(2,1)} fusion(bf16[129,2048]{1,0:T(8,128)(2,1)S(1)} %concatenate.17, s32[1024]{0:T(1024)S(1)} %pad_clamp_fusion.1), kind=kCustom, calls=%fused_computation.1 | custom fusion | bytes 3147264 | tf_op jit(solution)/shard_map/gather | solution.py:151
  24.0 4.4 %all-to-all-start = ((bf16[8,48,2048]{2,1,0:T(8,128)(2,1)}), bf16[8,48,2048]{2,1,0:T(8,128)(2,1)}, u32[]{:S(2)}, u32[]{:S(2)}) async-start(bf16[8,48,2048]{2,1,0:T(8,128)(2,1)} %bitcast.21), calls=%async_computation.1 | async-start | bytes 3145728 | tf_op jit(solution)/shard_map/all_to_all | solution.py:152
  31.0 30.6 %collective-permute-done.1 = bf16[512,128]{0,1:T(8,128)(2,1)S(1)} collective-permute-done((bf16[512,128]{0,1:T(8,128)(2,1)S(1)}, bf16[512,128]{0,1:T(8,128)(2,1)S(1)}, u32[]{:S(2)}, u32[]{:S(2)}) %collective-permute-start.1) | collective-permute-done | bytes 131104 | tf_op jit(solution)/shard_map/ppermute | solution.py:24
  61.7 4.8 %collective-permute-start.5 = (bf16[512,128]{0,1:T(8,128)(2,1)S(1)}, bf16[512,128]{0,1:T(8,128)(2,1)S(1)}, u32[]{:S(2)}, u32[]{:S(2)}) collective-permute-start(bf16[512,128]{0,1:T(8,128)(2,1)S(1)} %collective-permute-done.4), channel_id=1, source_target_pairs={{4,0},{8,4},{12,8},{16,12},{20,16},{24,20},{28,24},{0,28},{5,1},{9... | collective-permute-start | bytes 393224 | tf_op jit(solution)/shard_map/ppermute | solution.py:26
  66.5 2.9 %collective-permute-done.2 = bf16[512,128]{0,1:T(8,128)(2,1)S(1)} collective-permute-done((bf16[512,128]{0,1:T(8,128)(2,1)S(1)}, bf16[512,128]{0,1:T(8,128)(2,1)S(1)}, u32[]{:S(2)}, u32[]{:S(2)}) %collective-permute-start.2) | collective-permute-done | bytes 131104 | tf_op jit(solution)/shard_map/ppermute | solution.py:24
  69.7 4.8 %collective-permute-start.6 = (bf16[512,128]{0,1:T(8,128)(2,1)S(1)}, bf16[512,128]{0,1:T(8,128)(2,1)S(1)}, u32[]{:S(2)}, u32[]{:S(2)}) collective-permute-start(bf16[512,128]{0,1:T(8,128)(2,1)S(1)} %collective-permute-done.5), channel_id=1, source_target_pairs={{4,0},{8,4},{12,8},{16,12},{20,16},{24,20},{28,24},{0,28},{5,1},{9... | collective-permute-start | bytes 393224 | tf_op jit(solution)/shard_map/ppermute | solution.py:26
  84.3 47.3 %while.13 = (s32[]{:T(128)}, f32[2048,64]{0,1:T(8,128)S(1)}, f32[2048]{0:T(1024)S(1)}, bf16[8,512,128]{1,2,0:T(8,128)(2,1)S(1)}, bf16[2048,64]{1,0:T(8,128)(2,1)S(1)}, /*index=5*/s32[]{:T(128)}, s32[]{:T(128)}) while((s32[]{:T(128)}, f32[2048,64]{0,1:T(8,128)S(1)}, f32[2048]{0:T(1024)S(1)}, bf16[8,512,128]{1,2,0:T(8,128)(2,1)S(1)}, ...), condition=%wide.region_4.5_spmd.clone, body=%wide.region_2.4_spmd.clone.sunk | while | flops 272893952 | bytes 10518620 | solution.py:127
  84.4 2.7 %fusion.74 = (f32[2048]{0:T(1024)S(1)}, f32[512,2048]{1,0:T(8,128)}) fusion(bf16[2048,64]{1,0:T(8,128)(2,1)S(1)} %get-tuple-element.147, bf16[512,128]{1,0:T(8,128)(2,1)S(1)} %bitcast.70), kind=kOutput, calls=%fused_computation.5.clone.1 | convolution fusion | flops 136312832 | bytes 4595712 | tf_op jit(solution)/shard_map/while/body/eval_jaxpr/qd,kd->qk/dot_general | solution.py:106
  87.1 3.1 %convolution_add_fusion.2 = f32[2048,64]{0,1:T(8,128)S(1)} fusion(f32[512,2048]{1,0:T(8,128)} %get-tuple-element.127, f32[2048,64]{0,1:T(8,128)S(1)} %get-tuple-element.137, pred[]{:T(512)S(6)} %compare.26, bf16[512,128]{1,0:T(8,128)(2,1)S(1)} %bitcast.71), kind=kOutput, calls=%fused_computation.7.clone.1 | convolution fusion | flops 136577024 | bytes 5373953 | tf_op jit(solution)/shard_map/while/body/eval_jaxpr/dot_general | solution.py:110
  90.4 2.7 %fusion.74 = (f32[2048]{0:T(1024)S(1)}, f32[512,2048]{1,0:T(8,128)}) fusion(bf16[2048,64]{1,0:T(8,128)(2,1)S(1)} %get-tuple-element.147, bf16[512,128]{1,0:T(8,128)(2,1)S(1)} %bitcast.70), kind=kOutput, calls=%fused_computation.5.clone.1 | convolution fusion | flops 136312832 | bytes 4595712 | tf_op jit(solution)/shard_map/while/body/eval_jaxpr/qd,kd->qk/dot_general | solution.py:106
  93.0 3.1 %convolution_add_fusion.2 = f32[2048,64]{0,1:T(8,128)S(1)} fusion(f32[512,2048]{1,0:T(8,128)} %get-tuple-element.127, f32[2048,64]{0,1:T(8,128)S(1)} %get-tuple-element.137, pred[]{:T(512)S(6)} %compare.26, bf16[512,128]{1,0:T(8,128)(2,1)S(1)} %bitcast.71), kind=kOutput, calls=%fused_computation.7.clone.1 | convolution fusion | flops 136577024 | bytes 5373953 | tf_op jit(solution)/shard_map/while/body/eval_jaxpr/dot_general | solution.py:110
  96.3 2.7 %fusion.74 = (f32[2048]{0:T(1024)S(1)}, f32[512,2048]{1,0:T(8,128)}) fusion(bf16[2048,64]{1,0:T(8,128)(2,1)S(1)} %get-tuple-element.147, bf16[512,128]{1,0:T(8,128)(2,1)S(1)} %bitcast.70), kind=kOutput, calls=%fused_computation.5.clone.1 | convolution fusion | flops 136312832 | bytes 4595712 | tf_op jit(solution)/shard_map/while/body/eval_jaxpr/qd,kd->qk/dot_general | solution.py:106
  98.9 3.1 %convolution_add_fusion.2 = f32[2048,64]{0,1:T(8,128)S(1)} fusion(f32[512,2048]{1,0:T(8,128)} %get-tuple-element.127, f32[2048,64]{0,1:T(8,128)S(1)} %get-tuple-element.137, pred[]{:T(512)S(6)} %compare.26, bf16[512,128]{1,0:T(8,128)(2,1)S(1)} %bitcast.71), kind=kOutput, calls=%fused_computation.7.clone.1 | convolution fusion | flops 136577024 | bytes 5373953 | tf_op jit(solution)/shard_map/while/body/eval_jaxpr/dot_general | solution.py:110
  102.2 2.7 %fusion.74 = (f32[2048]{0:T(1024)S(1)}, f32[512,2048]{1,0:T(8,128)}) fusion(bf16[2048,64]{1,0:T(8,128)(2,1)S(1)} %get-tuple-element.147, bf16[512,128]{1,0:T(8,128)(2,1)S(1)} %bitcast.70), kind=kOutput, calls=%fused_computation.5.clone.1 | convolution fusion | flops 136312832 | bytes 4595712 | tf_op jit(solution)/shard_map/while/body/eval_jaxpr/qd,kd->qk/dot_general | solution.py:106
  104.9 3.1 %convolution_add_fusion.2 = f32[2048,64]{0,1:T(8,128)S(1)} fusion(f32[512,2048]{1,0:T(8,128)} %get-tuple-element.127, f32[2048,64]{0,1:T(8,128)S(1)} %get-tuple-element.137, pred[]{:T(512)S(6)} %compare.26, bf16[512,128]{1,0:T(8,128)(2,1)S(1)} %bitcast.71), kind=kOutput, calls=%fused_computation.7.clone.1 | convolution fusion | flops 136577024 | bytes 5373953 | tf_op jit(solution)/shard_map/while/body/eval_jaxpr/dot_general | solution.py:110
  108.1 2.7 %fusion.74 = (f32[2048]{0:T(1024)S(1)}, f32[512,2048]{1,0:T(8,128)}) fusion(bf16[2048,64]{1,0:T(8,128)(2,1)S(1)} %get-tuple-element.147, bf16[512,128]{1,0:T(8,128)(2,1)S(1)} %bitcast.70), kind=kOutput, calls=%fused_computation.5.clone.1 | convolution fusion | flops 136312832 | bytes 4595712 | tf_op jit(solution)/shard_map/while/body/eval_jaxpr/qd,kd->qk/dot_general | solution.py:106
  110.8 3.1 %convolution_add_fusion.2 = f32[2048,64]{0,1:T(8,128)S(1)} fusion(f32[512,2048]{1,0:T(8,128)} %get-tuple-element.127, f32[2048,64]{0,1:T(8,128)S(1)} %get-tuple-element.137, pred[]{:T(512)S(6)} %compare.26, bf16[512,128]{1,0:T(8,128)(2,1)S(1)} %bitcast.71), kind=kOutput, calls=%fused_computation.7.clone.1 | convolution fusion | flops 136577024 | bytes 5373953 | tf_op jit(solution)/shard_map/while/body/eval_jaxpr/dot_general | solution.py:110
  114.0 2.7 %fusion.74 = (f32[2048]{0:T(1024)S(1)}, f32[512,2048]{1,0:T(8,128)}) fusion(bf16[2048,64]{1,0:T(8,128)(2,1)S(1)} %get-tuple-element.147, bf16[512,128]{1,0:T(8,128)(2,1)S(1)} %bitcast.70), kind=kOutput, calls=%fused_computation.5.clone.1 | convolution fusion | flops 136312832 | bytes 4595712 | tf_op jit(solution)/shard_map/while/body/eval_jaxpr/qd,kd->qk/dot_general | solution.py:106
  116.7 3.1 %convolution_add_fusion.2 = f32[2048,64]{0,1:T(8,128)S(1)} fusion(f32[512,2048]{1,0:T(8,128)} %get-tuple-element.127, f32[2048,64]{0,1:T(8,128)S(1)} %get-tuple-element.137, pred[]{:T(512)S(6)} %compare.26, bf16[512,128]{1,0:T(8,128)(2,1)S(1)} %bitcast.71), kind=kOutput, calls=%fused_computation.7.clone.1 | convolution fusion | flops 136577024 | bytes 5373953 | tf_op jit(solution)/shard_map/while/body/eval_jaxpr/dot_general | solution.py:110
  120.0 2.7 %fusion.74 = (f32[2048]{0:T(1024)S(1)}, f32[512,2048]{1,0:T(8,128)}) fusion(bf16[2048,64]{1,0:T(8,128)(2,1)S(1)} %get-tuple-element.147, bf16[512,128]{1,0:T(8,128)(2,1)S(1)} %bitcast.70), kind=kOutput, calls=%fused_computation.5.clone.1 | convolution fusion | flops 136312832 | bytes 4595712 | tf_op jit(solution)/shard_map/while/body/eval_jaxpr/qd,kd->qk/dot_general | solution.py:106
  122.6 3.1 %convolution_add_fusion.2 = f32[2048,64]{0,1:T(8,128)S(1)} fusion(f32[512,2048]{1,0:T(8,128)} %get-tuple-element.127, f32[2048,64]{0,1:T(8,128)S(1)} %get-tuple-element.137, pred[]{:T(512)S(6)} %compare.26, bf16[512,128]{1,0:T(8,128)(2,1)S(1)} %bitcast.71), kind=kOutput, calls=%fused_computation.7.clone.1 | convolution fusion | flops 136577024 | bytes 5373953 | tf_op jit(solution)/shard_map/while/body/eval_jaxpr/dot_general | solution.py:110
  125.9 2.7 %fusion.74 = (f32[2048]{0:T(1024)S(1)}, f32[512,2048]{1,0:T(8,128)}) fusion(bf16[2048,64]{1,0:T(8,128)(2,1)S(1)} %get-tuple-element.147, bf16[512,128]{1,0:T(8,128)(2,1)S(1)} %bitcast.70), kind=kOutput, calls=%fused_computation.5.clone.1 | convolution fusion | flops 136312832 | bytes 4595712 | tf_op jit(solution)/shard_map/while/body/eval_jaxpr/qd,kd->qk/dot_general | solution.py:106
  128.5 3.1 %convolution_add_fusion.2 = f32[2048,64]{0,1:T(8,128)S(1)} fusion(f32[512,2048]{1,0:T(8,128)} %get-tuple-element.127, f32[2048,64]{0,1:T(8,128)S(1)} %get-tuple-element.137, pred[]{:T(512)S(6)} %compare.26, bf16[512,128]{1,0:T(8,128)(2,1)S(1)} %bitcast.71), kind=kOutput, calls=%fused_computation.7.clone.1 | convolution fusion | flops 136577024 | bytes 5373953 | tf_op jit(solution)/shard_map/while/body/eval_jaxpr/dot_general | solution.py:110
  134.3 4.6 %fusion.12 = f32[384,1024]{1,0:T(8,128)S(1)} fusion(bf16[384,2048]{1,0:T(8,128)(2,1)} %bitcast.22, bf16[1,2048,1024]{2,1,0:T(8,128)(2,1)} %param.27), kind=kOutput, calls=%fused_computation.19 | convolution fusion | flops 1610612736 | bytes 7340032 | tf_op jit(solution)/shard_map/dot_general | solution.py:154
  138.9 3.5 %multiply_convert_fusion = bf16[384,1024]{1,0:T(8,128)(2,1)S(1)} fusion(f32[384,1024]{1,0:T(8,128)S(1)} %fusion.12, bf16[384,2048]{1,0:T(8,128)(2,1)} %bitcast.22, bf16[1,2048,1024]{2,1,0:T(8,128)(2,1)S(1)} %copy-done.7), kind=kOutput, calls=%fused_computation.23 | convolution fusion | flops 1612972032 | bytes 8126464 | tf_op jit(solution)/shard_map/dot_general | solution.py:155
  142.5 3.0 %fusion.14 = bf16[8,48,2048]{2,1,0:T(8,128)(2,1)} fusion(bf16[8,48,1024]{2,1,0:T(8,128)(2,1)S(1)} %bitcast.79, bf16[1,1024,2048]{2,1,0:T(8,128)(2,1)S(1)} %copy-done.8), kind=kOutput, calls=%fused_computation.22 | convolution fusion | flops 1611399168 | bytes 6553600 | tf_op jit(solution)/shard_map/dot_general | solution.py:157
  145.7 22.4 %reduce-scatter.3.cloned.1.call-done = bf16[128,2048]{1,0:T(8,128)(2,1)} async-done(((bf16[512,2048]{1,0:T(8,128)(2,1)}), bf16[128,2048]{1,0:T(8,128)(2,1)}) %reduce-scatter.3.cloned.1.call-update) | async-done | bytes 524304 | tf_op jit(solution)/shard_map/reduce_scatter | solution.py:132
  169.4 29.4 %reduce-scatter.5.cloned.1.call-done = bf16[8,48,512]{2,1,0:T(8,128)(2,1)} async-done(((bf16[8,48,2048]{2,1,0:T(8,128)(2,1)}), bf16[8,48,512]{2,1,0:T(8,128)(2,1)}) %reduce-scatter.5.cloned.1.call-update) | async-done | bytes 393232 | tf_op jit(solution)/shard_map/reduce_scatter | solution.py:159
  198.8 5.5 %all-to-all-start.1 = ((bf16[8,48,512]{2,1,0:T(8,128)(2,1)}), bf16[8,48,512]{2,1,0:T(8,128)(2,1)S(1)}, u32[]{:S(2)}, u32[]{:S(2)}) async-start(bf16[8,48,512]{2,1,0:T(8,128)(2,1)} %reduce-scatter.5.cloned.1.call-done), calls=%async_computation.3 | async-start | bytes 786432 | tf_op jit(solution)/shard_map/all_to_all | solution.py:162
  206.3 9.5 %all-to-all-done.1 = bf16[8,48,512]{2,1,0:T(8,128)(2,1)S(1)} async-done(((bf16[8,48,512]{2,1,0:T(8,128)(2,1)}), bf16[8,48,512]{2,1,0:T(8,128)(2,1)S(1)}, u32[]{:S(2)}, u32[]{:S(2)}) %all-to-all-start.1) | async-done | bytes 393248 | tf_op jit(solution)/shard_map/all_to_all | solution.py:162
  (123 shorter events, 30.1 us)
Async XLA Ops:
  7.2 124.8 %copy-start = (bf16[256,2048]{1,0:T(8,128)(2,1)S(1)}, bf16[256,2048]{1,0:T(8,128)(2,1)}, u32[]{:S(2)}) copy-start(bf16[256,2048]{1,0:T(8,128)(2,1)} %param.21) | copy-start | bytes 3145732
  7.2 13.2 %copy-start.1 = (bf16[128,2048]{1,0:T(8,128)(2,1)S(1)}, bf16[128,2048]{1,0:T(8,128)(2,1)}, u32[]{:S(2)}) copy-start(bf16[128,2048]{1,0:T(8,128)(2,1)} %param.23) | copy-start | bytes 1572868
  7.2 13.4 %copy-start.4 = (f32[2048]{0:T(1024)S(1)}, f32[2048]{0:T(1024)}, u32[]{:S(2)}) copy-start(f32[2048]{0:T(1024)} %param.26) | copy-start | bytes 24580
  9.8 19.0 %collective-permute-start = (bf16[512,128]{0,1:T(8,128)(2,1)S(1)}, bf16[512,128]{0,1:T(8,128)(2,1)S(1)}, u32[]{:S(2)}, u32[]{:S(2)}) collective-permute-start(bf16[512,128]{0,1:T(8,128)(2,1)S(1)} %pad_maximum_fusion), channel_id=1, source_target_pairs={{0,4},{4,8},{8,12},{12,16},{16,20},{20,24},{24,28},{28,0},{1,5},{5... | collective-permute-start | bytes 393224 | tf_op jit(solution)/shard_map/ppermute | solution.py:24
  12.9 48.9 %collective-permute-start.4 = (bf16[512,128]{0,1:T(8,128)(2,1)S(1)}, bf16[512,128]{0,1:T(8,128)(2,1)S(1)}, u32[]{:S(2)}, u32[]{:S(2)}) collective-permute-start(bf16[512,128]{0,1:T(8,128)(2,1)S(1)} %pad_maximum_fusion), channel_id=1, source_target_pairs={{4,0},{8,4},{12,8},{16,12},{20,16},{24,20},{28,24},{0,28},{5,1},{9... | collective-permute-start | bytes 393224 | tf_op jit(solution)/shard_map/ppermute | solution.py:26
  24.0 4.5 %copy-start.2 = (bf16[512,256]{1,0:T(8,128)(2,1)S(1)}, bf16[512,256]{1,0:T(8,128)(2,1)}, u32[]{:S(2)}) copy-start(bf16[512,256]{1,0:T(8,128)(2,1)} %param.16) | copy-start | bytes 786436
  24.0 4.7 %copy-start.6 = (f32[64]{0:T(128)S(1)}, f32[64]{0:T(128)}, u32[]{:S(2)}) copy-start(f32[64]{0:T(128)} %param.19) | copy-start | bytes 772
  24.0 110.3 %all-to-all-start = ((bf16[8,48,2048]{2,1,0:T(8,128)(2,1)}), bf16[8,48,2048]{2,1,0:T(8,128)(2,1)}, u32[]{:S(2)}, u32[]{:S(2)}) async-start(bf16[8,48,2048]{2,1,0:T(8,128)(2,1)} %bitcast.21), calls=%async_computation.1 | async-start | bytes 3145728 | tf_op jit(solution)/shard_map/all_to_all | solution.py:152
  28.4 139.8 %reduce-scatter.3.cloned.1.call-start = ((), (), s32[]{:S(2)}) async-start(), calls=%async_computation.4 | async-start | bytes 2621440 | tf_op jit(solution)/shard_map/reduce_scatter | solution.py:132
  28.8 32.8 %collective-permute-start.1 = (bf16[512,128]{0,1:T(8,128)(2,1)S(1)}, bf16[512,128]{0,1:T(8,128)(2,1)S(1)}, u32[]{:S(2)}, u32[]{:S(2)}) collective-permute-start(bf16[512,128]{0,1:T(8,128)(2,1)S(1)} %collective-permute-done), channel_id=1, source_target_pairs={{0,4},{4,8},{8,12},{12,16},{16,20},{20,24},{24,28},{28,0},{1,5},{5... | collective-permute-start | bytes 393224 | tf_op jit(solution)/shard_map/ppermute | solution.py:24
  61.6 7.8 %collective-permute-start.2 = (bf16[512,128]{0,1:T(8,128)(2,1)S(1)}, bf16[512,128]{0,1:T(8,128)(2,1)S(1)}, u32[]{:S(2)}, u32[]{:S(2)}) collective-permute-start(bf16[512,128]{0,1:T(8,128)(2,1)S(1)} %collective-permute-done.1), channel_id=1, source_target_pairs={{0,4},{4,8},{8,12},{12,16},{16,20},{20,24},{24,28},{28,0},{1,5},{5... | collective-permute-start | bytes 393224 | tf_op jit(solution)/shard_map/ppermute | solution.py:24
  61.7 8.0 %collective-permute-start.5 = (bf16[512,128]{0,1:T(8,128)(2,1)S(1)}, bf16[512,128]{0,1:T(8,128)(2,1)S(1)}, u32[]{:S(2)}, u32[]{:S(2)}) collective-permute-start(bf16[512,128]{0,1:T(8,128)(2,1)S(1)} %collective-permute-done.4), channel_id=1, source_target_pairs={{4,0},{8,4},{12,8},{16,12},{20,16},{24,20},{28,24},{0,28},{5,1},{9... | collective-permute-start | bytes 393224 | tf_op jit(solution)/shard_map/ppermute | solution.py:26
  69.4 7.8 %collective-permute-start.3 = (bf16[512,128]{0,1:T(8,128)(2,1)S(1)}, bf16[512,128]{0,1:T(8,128)(2,1)S(1)}, u32[]{:S(2)}, u32[]{:S(2)}) collective-permute-start(bf16[512,128]{0,1:T(8,128)(2,1)S(1)} %collective-permute-done.2), channel_id=1, source_target_pairs={{0,4},{4,8},{8,12},{12,16},{16,20},{20,24},{24,28},{28,0},{1,5},{5... | collective-permute-start | bytes 393224 | tf_op jit(solution)/shard_map/ppermute | solution.py:24
  69.7 12.0 %collective-permute-start.6 = (bf16[512,128]{0,1:T(8,128)(2,1)S(1)}, bf16[512,128]{0,1:T(8,128)(2,1)S(1)}, u32[]{:S(2)}, u32[]{:S(2)}) collective-permute-start(bf16[512,128]{0,1:T(8,128)(2,1)S(1)} %collective-permute-done.5), channel_id=1, source_target_pairs={{4,0},{8,4},{12,8},{16,12},{20,16},{24,20},{28,24},{0,28},{5,1},{9... | collective-permute-start | bytes 393224 | tf_op jit(solution)/shard_map/ppermute | solution.py:26
  134.1 64.7 %reduce-scatter.5.cloned.1.call-start = ((), (), s32[]{:S(2)}) async-start(), calls=%async_computation.5 | async-start | bytes 1966080 | tf_op jit(solution)/shard_map/reduce_scatter | solution.py:159
  134.3 4.6 %copy-start.7 = (bf16[1,2048,1024]{2,1,0:T(8,128)(2,1)S(1)}, bf16[1,2048,1024]{2,1,0:T(8,128)(2,1)}, u32[]{:S(2)}) copy-start(bf16[1,2048,1024]{2,1,0:T(8,128)(2,1)} %param.28) | copy-start | bytes 12582916
  138.9 3.6 %copy-start.8 = (bf16[1,1024,2048]{2,1,0:T(8,128)(2,1)S(1)}, bf16[1,1024,2048]{2,1,0:T(8,128)(2,1)}, u32[]{:S(2)}) copy-start(bf16[1,1024,2048]{2,1,0:T(8,128)(2,1)} %param.29) | copy-start | bytes 12582916
  142.5 3.0 %copy-start.3 = (f32[128,2]{0,1:T(2,128)S(1)}, f32[128,2]{0,1:T(2,128)}, u32[]{:S(2)}) copy-start(f32[128,2]{0,1:T(2,128)} %param.25) | copy-start | bytes 3076
  145.5 58.8 %copy-start.5 = (f32[2048]{0:T(1024)S(1)}, f32[2048]{0:T(1024)}, u32[]{:S(2)}) copy-start(f32[2048]{0:T(1024)} %param.22) | copy-start | bytes 24580
  198.8 17.1 %all-to-all-start.1 = ((bf16[8,48,512]{2,1,0:T(8,128)(2,1)}), bf16[8,48,512]{2,1,0:T(8,128)(2,1)S(1)}, u32[]{:S(2)}, u32[]{:S(2)}) async-start(bf16[8,48,512]{2,1,0:T(8,128)(2,1)} %reduce-scatter.5.cloned.1.call-done), calls=%async_computation.3 | async-start | bytes 786432 | tf_op jit(solution)/shard_map/all_to_all | solution.py:162
Sparse Core Ops, SparseCore 0:
  134.2 33.9 reduce-scatter.2
  170.7 28.0 reduce-scatter.4
